TPU v7x, 32 devices: a whole 2x2x4 slice. The times are simulated.
32 devices in a mesh: sp: 8 (over z, y), tp: 4 (over x, core).
Axes of the slice: x: 2, y: 2, z: 4, core: 2. Of those that a mesh axis runs over, the one named last changes fastest.
Arguments:
- residual: bfloat16 [2048, 2048], P('sp'), may hold values from -6 to 6
- queries: bfloat16 [2048, 8, 128], P('sp', 'tp'), may hold values from -100 to 100
- keys: bfloat16 [2048, 8, 128], P('sp', 'tp'), may hold values from -60 to 60
- values: bfloat16 [2048, 8, 128], P('sp', 'tp'), may hold values from -6 to 6
- documents: int32 [2048], P('sp'), may hold values from 0 to 7, never falling along the last dimension, each value on 1 to 1024 neighbouring positions
- lambdas: float32 [8], P('tp'), may hold values from 0.3 to 0.8
- head_gain: float32 [8, 128], P('tp'), may hold values from 0.1 to 1.9
- out_weight: bfloat16 [1024, 2048], replicated, may hold values from -0.1875 to 0.1875
- mix_gain: float32 [2048], replicated, may hold values from 0.1 to 1.9
- pre_gain: float32 [2048], replicated, may hold values from 0.1 to 1.9
- gate_weight: bfloat16 [2048, 3072], P('sp', 'tp'), may hold values from -0.125 to 0.125
- value_weight: bfloat16 [2048, 3072], P('sp', 'tp'), may hold values from -0.125 to 0.125
- gate_taps: float32 [3, 3072], P(None, 'tp'), may hold values from -3 to 3
- value_taps: float32 [3, 3072], P(None, 'tp'), may hold values from -3 to 3
- down_weight: bfloat16 [2048, 3072], P('sp', 'tp'), may hold values from -0.109375 to 0.109375
- mlp_gain: float32 [2048], replicated, may hold values from 0.1 to 1.9
Outputs:
- out: bfloat16 [2048, 2048], P('sp')
All inputs are finite; a program needn't handle non-finite values.
Results may differ from a plain program's by a relative error of at most 0.015.
Values may be sent and summed in bfloat16 or wider, within the bound.
A program may use at most 128 MiB of HBM per device.

v0:
```python
import math

import jax
import jax.numpy as jnp
from jax import lax
from jax.sharding import PartitionSpec as P

epsilon = 1e-06
masked_score = -1e30


def passed_along(array, axis, by):
    length = lax.axis_size(axis)
    pairs = [(i, i + by) for i in range(length) if 0 <= i + by < length]
    return lax.ppermute(array, axis, pairs)


def rms_scale(values_in, gain):
    return (
        values_in
        * lax.rsqrt(jnp.mean(values_in * values_in, axis=-1, keepdims=True) + epsilon)
        * gain
    )


def attend_keys(
    running, queries, query_docs, query_pos, key_rows, value_rows, key_docs, key_pos, score_scale
):
    allowed = (key_pos[None, :] <= query_pos[:, None]) & (key_docs[None, :] == query_docs[:, None])
    map_width = queries.shape[2] // 2
    updated = []
    for map_index in range(2):
        row_max, row_sum, weighted = running[map_index]
        first_col = map_index * map_width
        scores = (
            jnp.einsum(
                "qhd,khd->hqk",
                queries[:, :, first_col : first_col + map_width],
                key_rows[:, :, first_col : first_col + map_width],
                preferred_element_type=jnp.float32,
            )
            * score_scale
        )
        scores = jnp.where(allowed[None], scores, masked_score)
        new_max = jnp.maximum(row_max, jnp.max(scores, axis=2))
        probs = jnp.where(allowed[None], jnp.exp(scores - new_max[:, :, None]), 0.0)
        factor = jnp.exp(row_max - new_max)
        row_sum = row_sum * factor + jnp.sum(probs, axis=2)
        weighted = weighted * jnp.transpose(factor)[:, :, None] + jnp.einsum(
            "hqk,khe->qhe",
            probs.astype(jnp.bfloat16),
            value_rows,
            preferred_element_type=jnp.float32,
        )
        updated.append((new_max, row_sum, weighted))
    return tuple(updated)


def per_device(
    residual,
    queries,
    keys,
    values,
    documents,
    lambdas,
    head_gain,
    out_weight,
    mix_gain,
    pre_gain,
    gate_weight,
    value_weight,
    gate_taps,
    value_taps,
    down_weight,
    mlp_gain,
):
    tok_rows = residual.shape[0]
    local_heads = queries.shape[1]
    head_dim = values.shape[2]
    score_scale = (queries.shape[2] // 2) ** (-0.5)
    query_pos = lax.axis_index("sp") * tok_rows + jnp.arange(tok_rows, dtype=jnp.int32)
    last_query = query_pos[tok_rows - 1]
    one_map = (
        jnp.full((local_heads, tok_rows), masked_score, jnp.float32),
        jnp.zeros((local_heads, tok_rows), jnp.float32),
        jnp.zeros((tok_rows, local_heads, head_dim), jnp.float32),
    )
    initial = (one_map, one_map)
    pieces = (
        lax.all_gather(keys, "sp", axis=0, tiled=True),
        lax.all_gather(values, "sp", axis=0, tiled=True),
        lax.all_gather(documents, "sp", axis=0, tiled=True),
    )
    length = pieces[0].shape[0]
    key_block = math.gcd(length, 1024)

    def advance(number, carried):
        offset = number * key_block

        def compute(state):
            key_rows = lax.dynamic_slice_in_dim(pieces[0], offset, key_block, 0)
            value_rows = lax.dynamic_slice_in_dim(pieces[1], offset, key_block, 0)
            key_docs = lax.dynamic_slice_in_dim(pieces[2], offset, key_block, 0)
            key_pos = offset + jnp.arange(key_block, dtype=jnp.int32)
            return attend_keys(
                state,
                queries,
                documents,
                query_pos,
                key_rows,
                value_rows,
                key_docs,
                key_pos,
                score_scale,
            )

        def passing(state):
            return state

        return lax.cond(offset <= last_query, compute, passing, carried)

    running = lax.fori_loop(0, length // key_block, advance, initial)
    outputs = [
        weighted / jnp.transpose(row_sum)[:, :, None] for row_max, row_sum, weighted in running
    ]
    heads = outputs[0] - lambdas[None, :, None] * outputs[1]
    normed = (
        rms_scale(heads, head_gain[None])
        .astype(jnp.bfloat16)
        .reshape(tok_rows, local_heads * head_dim)
    )
    weight_part = out_weight
    mixed = jnp.dot(
        lax.all_gather(normed, "tp", axis=1, tiled=True),
        weight_part,
        preferred_element_type=jnp.float32,
    )
    stream = residual.astype(jnp.float32) + rms_scale(mixed, mix_gain)
    normal_input = rms_scale(stream, pre_gain).astype(jnp.bfloat16)
    shard_rows = (
        lax.all_gather(gate_weight, "sp", axis=0, tiled=True),
        lax.all_gather(value_weight, "sp", axis=0, tiled=True),
    )
    gate_sum, value_sum = tuple(
        (
            jnp.dot(normal_input, weight_part, preferred_element_type=jnp.float32)
            for weight_part in shard_rows
        )
    )
    gate_pre = gate_sum.astype(jnp.bfloat16)
    value_pre = value_sum.astype(jnp.bfloat16)
    reach = gate_taps.shape[0] - 1
    rim_gate, rim_value, rim_docs = passed_along(
        (
            gate_pre[tok_rows - reach :],
            value_pre[tok_rows - reach :],
            documents[tok_rows - reach :],
        ),
        "sp",
        1,
    )
    earlier_docs = jnp.concatenate([rim_docs, documents])

    def convolve(rim_part, own_part, tap_rows):
        extended = lax.optimization_barrier(jnp.concatenate([rim_part, own_part])).astype(
            jnp.float32
        )
        summed = jnp.zeros(own_part.shape, jnp.float32)
        for shift_by in range(reach + 1):
            same_doc = (earlier_docs[shift_by : shift_by + tok_rows] == documents)[:, None]
            summed = summed + jnp.where(
                same_doc,
                tap_rows[shift_by][None, :] * extended[shift_by : shift_by + tok_rows],
                0.0,
            )
        return summed

    hidden = (
        jax.nn.gelu(convolve(rim_gate, gate_pre, gate_taps), approximate=True)
        * convolve(rim_value, value_pre, value_taps)
    ).astype(jnp.bfloat16)
    down_terms = lax.dot_general(
        hidden,
        lax.all_gather(down_weight, "sp", axis=0, tiled=True),
        (((1,), (1,)), ((), ())),
        preferred_element_type=jnp.float32,
    )
    lifted = lax.psum(down_terms.astype(jnp.bfloat16), "tp").astype(jnp.float32)
    return (stream + rms_scale(lifted, mlp_gain)).astype(jnp.bfloat16)


def solution(mesh):
    placed = (
        P("sp", None),
        P("sp", "tp", None),
        P("sp", "tp", None),
        P("sp", "tp", None),
        P("sp"),
        P("tp"),
        P("tp", None),
        P(),
        P(),
        P(),
        P("sp", "tp"),
        P("sp", "tp"),
        P(None, "tp"),
        P(None, "tp"),
        P("sp", "tp"),
        P(),
    )
    return jax.shard_map(
        per_device, mesh=mesh, in_specs=placed, out_specs=P("sp", None), check_vma=False
    )
```

profile of v0, /device:TPU:0, one launch (start us, length us, event | category | flops | bytes accessed | tf_op | source)
XLA Modules:
  0.0 327.3 jit_solution(7999324434239218202)
XLA Ops:
  6.5 1.7 copy.24
  8.3 0.0 all-gather.9.cloned.1.call-start
  8.3 1.7 copy.25
  10.0 0.0 all-gather.11.cloned.1.call-start
  10.1 0.7 all-gather.11.cloned.1.call-update
  10.8 0.0 all-gather.13.cloned.1.call-start
  10.8 0.5 all-gather.13.cloned.1.call-update
  11.4 0.5 all-gather.15.cloned.1.call-update
  12.0 0.8 slice.69
  12.7 4.9 %collective-permute-start = (s32[2]{0:T(128)S(1)}, s32[2]{0:T(128)S(1)}, u32[]{:S(2)}, u32[]{:S(2)}) collective-permute-start(s32[2]{0:T(128)S(1)} %slice.69), channel_id=1, source_target_pairs={{0,4},{4,8},{8,12},{12,16},{16,20},{20,24},{24,28},{1,5},{5,9},{9,... | collective-permute-start | bytes 32 | tf_op jit(solution)/shard_map/ppermute | solution.py:15
  17.6 0.6 slice.68
  18.3 1.0 copy.26
  19.3 18.7 %all-gather = s32[8,1,256]{2,1,0:T(1,128)S(1)} all-gather(s32[1,1,256]{2,1,0:T(1,128)S(1)} %bitcast.49), channel_id=1, replica_groups=mesh['sp'=8,'tp'=4] {'sp'}, dimensions={0}, use_global_device_ids=true | all-gather | bytes 9216 | tf_op jit(solution)/shard_map/all_gather | solution.py:92
  38.0 0.6 slice_reduce_fusion.2
  38.7 0.1 pad_add_fusion
  38.7 0.6 slice_compare_fusion.1
  39.4 12.2 %all-gather.7.cloned.1.call-done = bf16[2048,2,128]{0,2,1:T(8,128)(2,1)} async-done(((bf16[256,2,128]{0,2,1:T(8,128)(2,1)}), bf16[2048,2,128]{0,2,1:T(8,128)(2,1)}) %all-gather.7.cloned.1.call-update) | async-done | bytes 1048592 | tf_op jit(solution)/shard_map/all_gather | solution.py:90
  51.5 40.5 %all-gather.9.cloned.1.call-done = bf16[2048,2,128]{0,2,1:T(8,128)(2,1)} async-done(((bf16[256,2,128]{0,2,1:T(8,128)(2,1)}), bf16[2048,2,128]{0,2,1:T(8,128)(2,1)}) %all-gather.9.cloned.1.call-update) | async-done | bytes 1048592 | tf_op jit(solution)/shard_map/all_gather | solution.py:91
  92.1 7.5 %while.24 = (s32[]{:T(128)}, f32[2,256]{1,0:T(2,128)S(1)}, f32[2,256]{1,0:T(2,128)S(1)}, f32[256,2,128]{0,2,1:T(8,128)S(1)}, f32[2,256]{1,0:T(2,128)S(1)}, /*ind...) while((s32[]{:T(128)}, f32[2,256]{1,0:T(2,128)S(1)}, ...), condition=%wide.region_7.8_spmd.clone, body=%wide.region_0.7_spmd.clone.sunk | while | flops 417337600 | bytes 23029232 | solution.py:122
  92.8 6.2 %conditional.3 = ((f32[2,256]{1,0:T(2,128)S(1)}, f32[2,256]{1,0:T(2,128)S(1)}, f32[256,2,128]{0,2,1:T(8,128)S(1)}, f32[2,256]{1,0:T(2,128)S(1)}, f32[2,256]{1,0:T(2,128)S(1)}, /*index=5*/f32[256,2,128]{0,2,1:T(8,128)S(1)})) conditional(s32[]{:T(128)} %convert_element_type.94, (f32[2,256]{1,0:T(2,128)S(1)}, f32[2,256]{1,0:T(2,128)S(1)}, ...), branch_computations={%region_1.0_spmd, %region_2.6_spmd} | conditional | flops 417337600 | bytes 23027874 | solution.py:120
  92.9 0.3 compare_and_fusion
  93.2 1.5 fusion.24
  94.7 1.8 fusion.3
  96.5 0.7 fusion.8
  97.2 0.7 fusion.9
  97.9 1.0 fusion.7
  99.7 0.1 multiply_reduce_fusion.2
  99.8 0.1 multiply_convert_fusion.1
  99.9 7.3 %all_gather.24 = bf16[256,1024]{0,1:T(8,128)(2,1)S(1)} all-gather(bf16[256,256]{0,1:T(8,128)(2,1)S(1)} %bitcast.45), channel_id=1, replica_groups=mesh['sp'=8,'tp'=4] {'tp'}, dimensions={1}, use_global_device_ids=true | all-gather | bytes 655360 | tf_op jit(solution)/shard_map/all_gather | solution.py:134
  107.2 3.7 %multiply_reduce_fusion.1 = (f32[256]{0:T(256)S(1)}, f32[256,2048]{1,0:T(8,128)S(1)}) fusion(bf16[256,1024]{0,1:T(8,128)(2,1)S(1)} %all_gather.24, bf16[1024,2048]{1,0:T(8,128)(2,1)} %param.27), kind=kOutput, calls=%fused_computation.60 | convolution fusion | flops 1074790144 | bytes 6816768 | tf_op jit(solution)/shard_map/dot_general | solution.py:133
  110.9 0.6 multiply_reduce_fusion
  111.4 0.6 add_rsqrt_fusion.2
  112.0 41.3 %all-gather.11.cloned.1.call-done = bf16[2048,768]{1,0:T(8,128)(2,1)} async-done(((bf16[256,768]{1,0:T(8,128)(2,1)}), bf16[2048,768]{1,0:T(8,128)(2,1)}) %all-gather.11.cloned.1.call-update) | async-done | bytes 3145744 | tf_op jit(solution)/shard_map/all_gather | solution.py:141
  153.3 3.1 convolution_convert_fusion.2
  156.5 0.6 slice.86
  157.1 3.0 collective-permute-start.1
  160.1 54.0 %all-gather.13.cloned.1.call-done = bf16[2048,768]{1,0:T(8,128)(2,1)} async-done(((bf16[256,768]{1,0:T(8,128)(2,1)}), bf16[2048,768]{1,0:T(8,128)(2,1)}) %all-gather.13.cloned.1.call-update) | async-done | bytes 3145744 | tf_op jit(solution)/shard_map/all_gather | solution.py:142
  214.1 3.1 convolution_convert_fusion.1
  217.3 2.6 collective-permute-start.2
  219.9 0.8 pad_maximum_fusion
  220.7 0.9 convert_element_type.50
  221.6 0.1 pad_maximum_fusion.1
  221.8 0.9 convert_element_type.52
  222.7 52.1 %all-gather.15.cloned.1.call-done = bf16[2048,768]{1,0:T(8,128)(2,1)} async-done(((bf16[256,768]{1,0:T(8,128)(2,1)}), bf16[2048,768]{1,0:T(8,128)(2,1)}) %all-gather.15.cloned.1.call-update) | async-done | bytes 3145744 | tf_op jit(solution)/shard_map/all_gather | solution.py:184
  274.8 6.0 %convolution_convert_fusion = bf16[256,2048]{1,0:T(8,128)(2,1)} fusion(bf16[2048,768]{1,0:T(8,128)(2,1)} %all-gather.15.cloned.1.call-done, f32[258,768]{1,0:T(8,128)} %convert_element_type.52, f32[258,768]{1,0:T(8,128)} %convert_element_type.50, f32[768]{0:T(1024)} %get-tuple-element.386, f32[768]{0:T(1024)} %get-tuple-element.387, ...), kind=kOutput, calls=%fused_computation.52 | convolution fusion | flops 810549248 | bytes 8937472 | tf_op jit(solution)/shard_map/dot_general | solution.py:182
  280.9 35.1 %all-reduce.2.cloned.1.call-done = bf16[256,2048]{1,0:T(8,128)(2,1)} async-done(((bf16[256,2048]{1,0:T(8,128)(2,1)}), bf16[256,2048]{1,0:T(8,128)(2,1)}) %all-reduce.2.cloned.1.call-update) | async-done | bytes 1048592 | tf_op jit(solution)/shard_map/psum | solution.py:188
  316.0 1.5 fusion.40
  317.5 2.9 fusion.43
  (49 shorter events, 0.3 us)
Async XLA Ops:
  6.5 12.8 %copy-start.1 = (s32[256]{0:T(256)S(1)}, s32[256]{0:T(256)}, u32[]{:S(2)}) copy-start(s32[256]{0:T(256)} %param.24) | copy-start | bytes 3076
  6.5 31.5 %copy-start.5 = (f32[3,768]{1,0:T(4,128)S(1)}, f32[3,768]{1,0:T(4,128)}, u32[]{:S(2)}) copy-start(f32[3,768]{1,0:T(4,128)} %param.32) | copy-start | bytes 27652
  6.5 31.5 %copy-start.4 = (f32[3,768]{1,0:T(4,128)S(1)}, f32[3,768]{1,0:T(4,128)}, u32[]{:S(2)}) copy-start(f32[3,768]{1,0:T(4,128)} %param.33) | copy-start | bytes 27652
  6.5 45.0 %all-gather.7.cloned.1.call-start = ((), (), s32[]{:S(2)}) async-start(), calls=%async_computation | async-start | bytes 1179648 | tf_op jit(solution)/shard_map/all_gather | solution.py:90
  8.3 83.8 %all-gather.9.cloned.1.call-start = ((), (), s32[]{:S(2)}) async-start(), calls=%async_computation.1 | async-start | bytes 1179648 | tf_op jit(solution)/shard_map/all_gather | solution.py:91
  10.0 143.3 %all-gather.11.cloned.1.call-start = ((), (), s32[]{:S(2)}) async-start(), calls=%async_computation.2 | async-start | bytes 3538944 | tf_op jit(solution)/shard_map/all_gather | solution.py:141
  10.8 203.3 %all-gather.13.cloned.1.call-start = ((), (), s32[]{:S(2)}) async-start(), calls=%async_computation.3 | async-start | bytes 3538944 | tf_op jit(solution)/shard_map/all_gather | solution.py:142
  11.3 263.5 %all-gather.15.cloned.1.call-start = ((), (), s32[]{:S(2)}) async-start(), calls=%async_computation.4 | async-start | bytes 3538944 | tf_op jit(solution)/shard_map/all_gather | solution.py:184
  11.9 304.1 %all-reduce.2.cloned.1.call-start = ((), (), s32[]{:S(2)}) async-start(), calls=%async_computation.5 | async-start | bytes 2097152 | tf_op jit(solution)/shard_map/psum | solution.py:188
  12.7 26.0 %collective-permute-start = (s32[2]{0:T(128)S(1)}, s32[2]{0:T(128)S(1)}, u32[]{:S(2)}, u32[]{:S(2)}) collective-permute-start(s32[2]{0:T(128)S(1)} %slice.69), channel_id=1, source_target_pairs={{0,4},{4,8},{8,12},{12,16},{16,20},{20,24},{24,28},{1,5},{5,9},{9,... | collective-permute-start | bytes 32 | tf_op jit(solution)/shard_map/ppermute | solution.py:15
  92.1 7.5 %copy-start.7 = (f32[2]{0:T(128)S(1)}, f32[2]{0:T(128)}, u32[]{:S(2)}) copy-start(f32[2]{0:T(128)} %param.25) | copy-start | bytes 28
  92.1 7.7 %copy-start.6 = (f32[2,128]{1,0:T(2,128)S(1)}, f32[2,128]{1,0:T(2,128)}, u32[]{:S(2)}) copy-start(f32[2,128]{1,0:T(2,128)} %param.26) | copy-start | bytes 3076
  94.7 1.8 copy-start.8
  107.2 3.7 %copy-start = (bf16[256,2048]{1,0:T(8,128)(2,1)S(1)}, bf16[256,2048]{1,0:T(8,128)(2,1)}, u32[]{:S(2)}) copy-start(bf16[256,2048]{1,0:T(8,128)(2,1)} %param.20) | copy-start | bytes 3145732
  107.2 3.7 %copy-start.2 = (f32[2048]{0:T(1024)S(1)}, f32[2048]{0:T(1024)}, u32[]{:S(2)}) copy-start(f32[2048]{0:T(1024)} %param.28) | copy-start | bytes 24580
  157.1 62.8 %collective-permute-start.1 = (bf16[2,768]{1,0:T(2,128)(2,1)}, bf16[2,768]{1,0:T(2,128)(2,1)}, u32[]{:S(2)}, u32[]{:S(2)}) collective-permute-start(bf16[2,768]{1,0:T(2,128)(2,1)} %slice.86), channel_id=1, source_target_pairs={{0,4},{4,8},{8,12},{12,16},{16,20},{20,24},{24,28},{1,5},{5,9},{9,... | collective-permute-start | bytes 9224 | tf_op jit(solution)/shard_map/ppermute | solution.py:15
  217.3 4.4 %collective-permute-start.2 = (bf16[2,768]{1,0:T(2,128)(2,1)S(1)}, bf16[2,768]{1,0:T(2,128)(2,1)S(1)}, u32[]{:S(2)}, u32[]{:S(2)}) collective-permute-start(bf16[2,768]{1,0:T(2,128)(2,1)S(1)} %slice.90), channel_id=1, source_target_pairs={{0,4},{4,8},{8,12},{12,16},{16,20},{20,24},{24,28},{1,5},{5,9},{9,... | collective-permute-start | bytes 9224 | tf_op jit(solution)/shard_map/ppermute | solution.py:15
  280.9 36.6 %copy-start.3 = (f32[2048]{0:T(1024)S(1)}, f32[2048]{0:T(1024)}, u32[]{:S(2)}) copy-start(f32[2048]{0:T(1024)} %param.35) | copy-start | bytes 24580
Sparse Core Ops, SparseCore 0:
  9.4 42.1 all-gather.6
  53.6 38.3 all-gather.8
  94.2 59.0 all-gather.10
  155.4 58.6 all-gather.12
  216.1 58.6 all-gather.14
  281.0 34.9 all-reduce.1
where the time goes:
time: 328 us; the launch traced here: 327 us
  waiting for transfers between devices  237 us (72%)
  blocking collectives  26 us (8%)
  matrix products  20.6 us (6%)
  between operations  13.7 us (4%)
  starting transfers between devices  10.8 us (3%)
  other arithmetic  10.7 us (3%)
  local copies, waits for them, and re-layouts  7.13 us (2%)
    all_gather x1, waiting for transfers between devices, per_device(): lax.all_gather(value_weight, 'sp', axis=0, tiled=True)  54 us
    all_gather x1, waiting for transfers between devices, per_device(): lax.all_gather(down_weight, 'sp', axis=0, tiled=True)  52.1 us
    all_gather x1, waiting for transfers between devices, per_device(): lax.all_gather(gate_weight, 'sp', axis=0, tiled=True)  41.3 us
    all_gather x1, waiting for transfers between devices, per_device(): lax.all_gather(values, 'sp', axis=0, tiled=True)  40.5 us
    psum x1, waiting for transfers between devices, per_device(): lifted = lax.psum(down_terms.astype(jnp.bfloat16), 'tp').astype(jnp.float32)  35.1 us
    all_gather x1, blocking collectives, per_device(): lax.all_gather(documents, 'sp', axis=0, tiled=True)  18.7 us
    all_gather x1, waiting for transfers between devices, per_device(): lax.all_gather(keys, 'sp', axis=0, tiled=True)  12.2 us
    ppermute x3, starting transfers between devices, passed_along(): return lax.ppermute(array, axis, pairs)  10.6 us
  transfers between devices with their start and end apart: 9, of which 6 were waited for; matrix products, arithmetic and copies ran while one was open for 8% of the time, Pallas kernels for 0%

commit v1 on v0

v1 whole, which is shorter than its diff:
```python
import functools

import jax
import jax.numpy as jnp
from jax import lax
from jax.experimental import pallas as pl
from jax.experimental.pallas import tpu as pltpu
from jax.sharding import PartitionSpec as P

epsilon = 1e-06
masked_score = -1e30
EXTRA = 32
KV, GATE, VALUE, DOWN = range(4)


def kernel(
    n,
    ntp,
    lam_ref,
    kv_hbm,
    g_hbm,
    v_hbm,
    d_hbm,
    ow_hbm,
    res_hbm,
    q_ref,
    dcol_ref,
    hg_ref,
    mixg_ref,
    preg_ref,
    gt_ref,
    vt_ref,
    mlpg_ref,
    out_ref,
    kvb,
    gb,
    vb,
    db,
    owb,
    resb,
    nrm,
    stream,
    xn,
    gacc,
    vacc,
    gext,
    vext,
    halo_out,
    halo_in,
    hidden,
    part,
    rsb,
    mrow,
    lrow,
    att,
    local_sem,
    ring_send,
    ring_recv,
    nrm_send,
    nrm_recv,
    halo_send,
    halo_recv,
    rs_send,
    rs_recv,
    ag_send,
    ag_recv,
):
    s = lax.axis_index("sp")
    t = lax.axis_index("tp")
    half = n // 2
    tok = resb.shape[0]
    width = resb.shape[1]
    rows = g_hbm.shape[0]
    ff = g_hbm.shape[1]
    heads = hg_ref.shape[0]
    hd = hg_ref.shape[1]
    hw = heads * hd
    share = tok // ntp
    pos = jnp.where(s % 2 == 0, s // 2, n - 1 - s // 2)

    def at(p):
        p = (p + n) % n
        return jnp.where(p < half, 2 * p, 2 * n - 1 - 2 * p)

    neighbour = (at(pos + 1), at(pos - 1))

    def place(kind, owner, piece):
        if kind == KV:
            size = kvb.shape[1]
            if piece is None:
                return kvb.at[owner]
            return kvb.at[owner, pl.ds(piece * (size // 2), size // 2)]
        ref = (None, gb, vb, db)[kind]
        if piece is None:
            return ref.at[pl.ds(pl.multiple_of(owner * rows, rows), rows)]
        return ref.at[pl.ds(pl.multiple_of(owner * rows + piece * (rows // 2), rows // 2), rows // 2)]

    def hop(kind, way, step, owner):
        ref = place(kind, owner, way if step == half else None)
        return pltpu.make_async_remote_copy(
            src_ref=ref,
            dst_ref=ref,
            send_sem=ring_send.at[kind, way, step - 1],
            recv_sem=ring_recv.at[kind, way, step - 1],
            device_id={"sp": neighbour[way]},
            device_id_type=pl.DeviceIdType.MESH,
        )

    def came(way, step):
        return at(pos - step) if way == 0 else at(pos + step)

    def send(kind, way, step):
        hop(kind, way, step, came(way, step - 1)).start()

    def arrive(kind, way, step):
        hop(kind, way, step, came(way, step)).wait_recv()

    local = [
        pltpu.make_async_copy(src, dst, local_sem.at[i])
        for i, (src, dst) in enumerate(
            (
                (kv_hbm, kvb.at[s]),
                (g_hbm, place(GATE, s, None)),
                (v_hbm, place(VALUE, s, None)),
                (d_hbm, place(DOWN, s, None)),
                (ow_hbm, owb),
                (res_hbm, resb),
            )
        )
    ]
    for copy in local:
        copy.start()
    local[0].wait()
    for way in range(2):
        send(KV, way, 1)
    for step in range(1, half):
        for way in range(2):
            arrive(KV, way, step)
            send(KV, way, step + 1)
    for i in (1, 2, 3):
        local[i].wait()
    for kind in (GATE, VALUE, DOWN):
        for way in range(2):
            send(kind, way, 1)
    for way in range(2):
        arrive(KV, way, half)

    mrow[...] = jnp.full(mrow.shape, masked_score, jnp.float32)
    lrow[...] = jnp.zeros(lrow.shape, jnp.float32)
    att[...] = jnp.zeros(att.shape, jnp.float32)
    doc_query = dcol_ref[:, 0:1]
    lane = lax.broadcasted_iota(jnp.int32, (tok, hd), 1)
    delta = lax.broadcasted_iota(jnp.int32, (tok, tok), 0) - lax.broadcasted_iota(
        jnp.int32, (tok, tok), 1
    )

    @pl.loop(0, jnp.minimum(s, half) + 1)
    def _(back):
        o = s - back
        doc_key = kvb[o, pl.ds(tok, 16), pl.ds(0, tok)].astype(jnp.float32)[0:1]
        allowed = (delta + back * tok >= 0) & (doc_key == doc_query)
        for h in range(heads):
            k = kvb[o, pl.ds(0, tok), pl.ds(h * hd, hd)]
            val = kvb[o, pl.ds(0, tok), pl.ds(hw + h * hd, hd)]
            qh = q_ref[:, h * hd : (h + 1) * hd]
            for m in range(2):
                keep = lane < hd // 2 if m == 0 else lane >= hd // 2
                qm = jnp.where(keep, qh, jnp.zeros_like(qh))
                scores = lax.dot_general(
                    qm, k, (((1,), (1,)), ((), ())), preferred_element_type=jnp.float32
                )
                scores = jnp.where(allowed, scores, masked_score)
                idx = h * 2 + m
                old = mrow[idx, :, 0:1]
                new = jnp.maximum(old, jnp.max(scores, axis=1, keepdims=True))
                probs = jnp.where(allowed, jnp.exp(scores - new), 0.0)
                factor = jnp.exp(old - new)
                total = lrow[idx, :, 0:1] * factor + jnp.sum(probs, axis=1, keepdims=True)
                att[idx] = att[idx] * factor + jnp.dot(
                    probs.astype(jnp.bfloat16), val, preferred_element_type=jnp.float32
                )
                mrow[idx] = jnp.broadcast_to(new, (tok, hd))
                lrow[idx] = jnp.broadcast_to(total, (tok, hd))

    for h in range(heads):
        head = att[2 * h] / lrow[2 * h] - lam_ref[h] * (att[2 * h + 1] / lrow[2 * h + 1])
        scale = lax.rsqrt(jnp.mean(head * head, axis=1, keepdims=True) + epsilon)
        nrm[t, :, pl.ds(h * hd, hd)] = (head * scale * hg_ref[h : h + 1, :]).astype(jnp.bfloat16)

    def peer_copy(src, dst, send_sem, recv_sem, i):
        return pltpu.make_async_remote_copy(
            src_ref=src,
            dst_ref=dst,
            send_sem=send_sem,
            recv_sem=recv_sem,
            device_id={"tp": (t + i) % ntp},
            device_id_type=pl.DeviceIdType.MESH,
        )

    def nrm_copy(i, slot):
        return peer_copy(nrm.at[slot], nrm.at[slot], nrm_send.at[i], nrm_recv.at[i], i)

    for i in range(1, ntp):
        nrm_copy(i, t).start()
    local[4].wait()
    local[5].wait()
    for i in range(1, ntp):
        nrm_copy(i, (t - i + ntp) % ntp).wait_recv()

    tile = 256

    @pl.loop(0, width // tile)
    def _(c):
        cols = pl.ds(pl.multiple_of(c * tile, tile), tile)
        acc = jnp.zeros((tok, tile), jnp.float32)
        for j in range(ntp):
            acc = acc + jnp.dot(
                nrm[j], owb[pl.ds(j * hw, hw), cols], preferred_element_type=jnp.float32
            )
        stream[:, cols] = acc

    def rms(x, gain):
        return x * lax.rsqrt(jnp.mean(x * x, axis=1, keepdims=True) + epsilon) * gain

    chunk = 16

    @pl.loop(0, tok // chunk)
    def _(c):
        part_rows = pl.ds(pl.multiple_of(c * chunk, chunk), chunk)
        st = resb[part_rows].astype(jnp.float32) + rms(stream[part_rows], mixg_ref[...])
        stream[part_rows] = st
        xn[part_rows] = rms(st, preg_ref[...]).astype(jnp.bfloat16)

    fine = rows % 128 == 0

    def add_block(kind, owner, first):
        acc, w = (gacc, gb) if kind == GATE else (vacc, vb)
        at_rows = pl.ds(pl.multiple_of(owner * rows, rows), rows)
        got = jnp.dot(xn[:, at_rows], w[at_rows, :], preferred_element_type=jnp.float32)
        if first:
            acc[...] = got
        else:
            acc[...] += got

    if fine:
        for kind in (GATE, VALUE):
            add_block(kind, s, True)
    for step in range(1, half + 1):
        for kind in (GATE, VALUE):
            for way in range(2):
                arrive(kind, way, step)
                if step < half:
                    send(kind, way, step + 1)
            if step == half and kind == VALUE:
                for way in range(2):
                    arrive(DOWN, way, 1)
                    send(DOWN, way, 2)
            if fine:
                add_block(kind, came(0, step), False)
                if step < half:
                    add_block(kind, came(1, step), False)
    if not fine:
        gacc[...] = jnp.dot(xn[...], gb[...], preferred_element_type=jnp.float32)
        vacc[...] = jnp.dot(xn[...], vb[...], preferred_element_type=jnp.float32)

    for i, (acc, ext) in enumerate(((gacc, gext), (vacc, vext))):
        ext[pl.ds(8, tok), :] = acc[...].astype(jnp.bfloat16).astype(jnp.float32)
        halo_out[i] = acc[pl.ds(tok - 16, 16), :].astype(jnp.bfloat16)
        ext[pl.ds(0, 8), :] = jnp.zeros((8, ff), jnp.float32)

    def halo(target):
        return pltpu.make_async_remote_copy(
            src_ref=halo_out,
            dst_ref=halo_in,
            send_sem=halo_send,
            recv_sem=halo_recv,
            device_id={"sp": target},
            device_id_type=pl.DeviceIdType.MESH,
        )

    @pl.when(s < n - 1)
    def _():
        halo(s + 1).start()

    @pl.when(s > 0)
    def _():
        halo(s - 1).wait_recv()
        for i, ext in enumerate((gext, vext)):
            ext[pl.ds(0, 8), :] = halo_in[i].astype(jnp.float32)[8:16]

    before = jnp.maximum(s - 1, 0)
    prev_docs = kvb[before, pl.ds(tok, 16), pl.ds(0, tok)].astype(jnp.float32)[0:1]
    lane_row = lax.broadcasted_iota(jnp.int32, (1, tok), 1)
    last1 = jnp.sum(jnp.where(lane_row == tok - 1, prev_docs, 0.0), axis=1, keepdims=True)
    last2 = jnp.sum(jnp.where(lane_row == tok - 2, prev_docs, 0.0), axis=1, keepdims=True)
    has_prev = s > 0
    last1 = jnp.where(has_prev, last1, -1.0)
    last2 = jnp.where(has_prev, last2, -1.0)
    rowid = lax.broadcasted_iota(jnp.int32, (tok, 1), 0)
    doc1 = jnp.where(rowid == 0, last1, dcol_ref[:, 1:2])
    doc2 = jnp.where(rowid == 0, last2, jnp.where(rowid == 1, last1, dcol_ref[:, 2:3]))
    same1 = doc1 == doc_query
    same2 = doc2 == doc_query

    @pl.loop(0, ff // 128)
    def _(c):
        cols = pl.ds(pl.multiple_of(c * 128, 128), 128)

        def conv(ext, taps):
            w = taps[:, cols]
            total = jnp.where(same2, w[0:1] * ext[pl.ds(6, tok), cols], 0.0)
            total = total + jnp.where(same1, w[1:2] * ext[pl.ds(7, tok), cols], 0.0)
            return total + w[2:3] * ext[pl.ds(8, tok), cols]

        hidden[:, cols] = (
            jax.nn.gelu(conv(gext, gt_ref), approximate=True) * conv(vext, vt_ref)
        ).astype(jnp.bfloat16)

    def rs_copy(i, b, cols):
        peer = (t + i) % ntp
        return peer_copy(
            part.at[pl.ds(pl.multiple_of(peer * share, share), share), cols],
            rsb.at[i - 1, :, cols],
            rs_send.at[b, i],
            rs_recv.at[b, i],
            i,
        )

    def block_cols(owner):
        return pl.ds(pl.multiple_of(owner * rows, rows), rows)

    def down_block(owner, b):
        cols = block_cols(owner)
        part[:, cols] = lax.dot_general(
            hidden[...], db[cols, :], (((1,), (1,)), ((), ())), preferred_element_type=jnp.float32
        ).astype(jnp.bfloat16)
        for i in range(1, ntp):
            rs_copy(i, b, cols).start()

    order = [s]
    if fine:
        down_block(s, 0)
    for step in range(1, half + 1):
        for way in range(2):
            if step > 1:
                arrive(DOWN, way, step)
                if step < half:
                    send(DOWN, way, step + 1)
        for way in range(2 if step < half else 1):
            if fine:
                down_block(came(way, step), len(order))
                order.append(came(way, step))
    if fine:
        pieces = [(b, block_cols(o)) for b, o in enumerate(order)]
    else:

        @pl.loop(0, width // tile)
        def _(c):
            cols = pl.ds(pl.multiple_of(c * tile, tile), tile)
            part[:, cols] = lax.dot_general(
                hidden[...],
                db[cols, :],
                (((1,), (1,)), ((), ())),
                preferred_element_type=jnp.float32,
            ).astype(jnp.bfloat16)

        pieces = [(0, pl.ds(0, width))]
        for i in range(1, ntp):
            rs_copy(i, 0, pieces[0][1]).start()
    for b, cols in pieces:
        for i in range(1, ntp):
            rs_copy(i, b, cols).wait_recv()

    mine = pl.multiple_of(t * share, share)

    @pl.loop(0, share // chunk)
    def _(c):
        at_rows = pl.ds(pl.multiple_of(mine + c * chunk, chunk), chunk)
        in_rows = pl.ds(pl.multiple_of(c * chunk, chunk), chunk)
        lifted = part[at_rows].astype(jnp.float32)
        for i in range(1, ntp):
            lifted = lifted + rsb[i - 1, in_rows].astype(jnp.float32)
        out_ref[at_rows] = (stream[at_rows] + rms(lifted, mlpg_ref[...])).astype(jnp.bfloat16)

    def ag_copy(i, owner):
        ref = out_ref.at[pl.ds(pl.multiple_of(owner * share, share), share)]
        return peer_copy(ref, ref, ag_send.at[i], ag_recv.at[i], i)

    for i in range(1, ntp):
        ag_copy(i, t).start()
    for i in range(1, ntp):
        ag_copy(i, (t - i + ntp) % ntp).wait_recv()

    for kind in (KV, GATE, VALUE, DOWN):
        for way in range(2):
            for step in range(1, half + 1):
                hop(kind, way, step, came(way, step - 1)).wait_send()
    for i in range(1, ntp):
        nrm_copy(i, t).wait_send()
        for b, cols in pieces:
            rs_copy(i, b, cols).wait_send()
        ag_copy(i, t).wait_send()

    @pl.when(s < n - 1)
    def _():
        halo(s + 1).wait_send()


def per_device(
    n,
    ntp,
    residual,
    queries,
    keys,
    values,
    documents,
    lambdas,
    head_gain,
    out_weight,
    mix_gain,
    pre_gain,
    gate_weight,
    value_weight,
    gate_taps,
    value_taps,
    down_weight,
    mlp_gain,
):
    tok, width = residual.shape
    heads, hd = head_gain.shape
    hw = heads * hd
    rows, ff = gate_weight.shape
    half = n // 2
    share = tok // ntp
    docs = documents.astype(jnp.float32)
    packed = jnp.concatenate([keys.reshape(tok, hw), values.reshape(tok, hw)], axis=1)
    doc_rows = jnp.broadcast_to(
        jnp.pad(docs, (0, 2 * hw - tok)).astype(jnp.bfloat16)[None, :], (EXTRA, 2 * hw)
    )
    kv = jnp.concatenate([packed, doc_rows], axis=0)
    back = [jnp.concatenate([jnp.full((j,), -1.0, jnp.float32), docs[: tok - j]]) for j in (1, 2)]
    dcol = jnp.pad(jnp.stack([docs] + back, axis=1), ((0, 0), (0, 125)))
    score_scale = (hd // 2) ** (-0.5)
    q = (queries.astype(jnp.float32) * score_scale).astype(jnp.bfloat16).reshape(tok, hw)
    bf, f32 = jnp.bfloat16, jnp.float32
    vm = pl.BlockSpec(memory_space=pltpu.VMEM)
    hbm = pl.BlockSpec(memory_space=pl.ANY)
    smem = pl.BlockSpec(memory_space=pltpu.SMEM)
    dma = pltpu.SemaphoreType.DMA
    return pl.pallas_call(
        functools.partial(kernel, n, ntp),
        out_shape=jax.ShapeDtypeStruct((tok, width), bf),
        in_specs=[smem] + [hbm] * 6 + [vm] * 8,
        out_specs=vm,
        scratch_shapes=[
            pltpu.VMEM((n, tok + EXTRA, 2 * hw), bf),
            pltpu.VMEM((n * rows, ff), bf),
            pltpu.VMEM((n * rows, ff), bf),
            pltpu.VMEM((n * rows, ff), bf),
            pltpu.VMEM(out_weight.shape, bf),
            pltpu.VMEM((tok, width), bf),
            pltpu.VMEM((ntp, tok, hw), bf),
            pltpu.VMEM((tok, width), f32),
            pltpu.VMEM((tok, width), bf),
            pltpu.VMEM((tok, ff), f32),
            pltpu.VMEM((tok, ff), f32),
            pltpu.VMEM((tok + 8, ff), f32),
            pltpu.VMEM((tok + 8, ff), f32),
            pltpu.VMEM((2, 16, ff), bf),
            pltpu.VMEM((2, 16, ff), bf),
            pltpu.VMEM((tok, ff), bf),
            pltpu.VMEM((tok, width), bf),
            pltpu.VMEM((ntp - 1, share, width), bf),
            pltpu.VMEM((2 * heads, tok, hd), f32),
            pltpu.VMEM((2 * heads, tok, hd), f32),
            pltpu.VMEM((2 * heads, tok, hd), f32),
            dma((6,)),
            dma((4, 2, half)),
            dma((4, 2, half)),
            dma((ntp,)),
            dma((ntp,)),
            dma,
            dma,
            dma((n, ntp)),
            dma((n, ntp)),
            dma((ntp,)),
            dma((ntp,)),
        ],
        compiler_params=pltpu.CompilerParams(
            has_side_effects=True, vmem_limit_bytes=60 * 1024 * 1024
        ),
    )(
        lambdas,
        kv,
        gate_weight,
        value_weight,
        down_weight,
        out_weight,
        residual,
        q,
        dcol,
        head_gain,
        mix_gain[None],
        pre_gain[None],
        gate_taps,
        value_taps,
        mlp_gain[None],
    )


def solution(mesh):
    placed = (
        P("sp", None),
        P("sp", "tp", None),
        P("sp", "tp", None),
        P("sp", "tp", None),
        P("sp"),
        P("tp"),
        P("tp", None),
        P(),
        P(),
        P(),
        P("sp", "tp"),
        P("sp", "tp"),
        P(None, "tp"),
        P(None, "tp"),
        P("sp", "tp"),
        P(),
    )
    body = functools.partial(per_device, mesh.shape["sp"], mesh.shape["tp"])
    return jax.shard_map(
        body, mesh=mesh, in_specs=placed, out_specs=P("sp", None), check_vma=False
    )
```

time: 328 us -> 167 us (0.51)
  waiting for transfers between devices: 237 us -> 0 us
  Pallas kernels: 0 us -> 158 us
  blocking collectives: 26 us -> 0 us
  matrix products: 20.6 us -> 0 us
  between operations: 13.7 us -> 0.03 us
  starting transfers between devices: 10.8 us -> 0 us
  other arithmetic: 10.7 us -> 2.53 us
    all_gather x5 -> x0, waiting for transfers between devices: 200 us -> none  [the longest x1 54 us: per_device(): lax.all_gather(value_weight, 'sp', axis=0, tiled=True)]
    pallas_call x0 -> x1, Pallas kernels: none -> 158 us  [per_device(): pl.pallas_call(functools.partial(kernel, n, ntp), out_shape=jax.ShapeDtyp...]
    psum x1 -> x0, waiting for transfers between devices: 35.1 us -> none  [per_device(): lifted = lax.psum(down_terms.astype(jnp.bfloat16), 'tp').astype(jnp.float32)]
    all_gather x2 -> x0, blocking collectives: 26 us -> none  [the longest x1 18.7 us: per_device(): lax.all_gather(documents, 'sp', axis=0, tiled=True)]
    dot_general x8 -> x0, matrix products: 20.6 us -> none  [the longest x2 6.29 us: per_device(): jnp.dot(normal_input, weight_part, preferred_element_type=jnp.float32)]
    ppermute x3 -> x0, starting transfers between devices: 10.6 us -> none  [passed_along(): return lax.ppermute(array, axis, pairs)]
  transfers between devices with their start and end apart: 9 -> 0, of which waited for: 6 -> 0; matrix products, arithmetic and copies ran while one was open for 8% -> 0% of each run, Pallas kernels for 0% -> 0%
where the time goes in v1:
time: 167 us; the launch traced here: 165 us
  Pallas kernels  158 us (95%)
  local copies, waits for them, and re-layouts  4.87 us (3%)
  other arithmetic  2.53 us (2%)
    pallas_call x1, Pallas kernels, per_device(): pl.pallas_call(functools.partial(kernel, n, ntp), out_shape=jax.ShapeDtyp...  158 us

profile of v1, /device:TPU:0, one launch (start us, length us, event | category | flops | bytes accessed | tf_op | source)
XLA Modules:
  0.0 165.4 jit_solution(17164165174973369894)
XLA Ops:
  0.0 0.7 fusion
  0.7 0.1 concatenate.15
  0.8 0.1 pad_maximum_fusion.2
  0.9 0.1 copy.20
  1.0 0.7 pad.11.dcol_ref
  1.7 1.0 multiply_convert_fusion
  2.7 0.7 copy.27
  3.4 1.0 copy_bitcast_fusion.1
  4.4 0.7 pad_maximum_fusion.kv_hbm
  5.1 157.9 %shard_map.154 = bf16[256,2048]{1,0:T(8,128)(2,1)} custom-call(f32[2]{0:T(128)} %lam_ref.1, bf16[288,512]{1,0:T(8,128)(2,1)} %pad_maximum_fusion.kv_hbm, bf16[256,768]{1,0:T(8,128)(2,1)} %g_hbm.1, bf16[256,768]{1,0:T(8,128)(2,1)} %v_hbm.1, bf16[256,768]{1,0:T(8,128)(2,1)} %d_hbm.1, bf16[1024,2048]{1,0:T(8,128)(2,1)} %ow_hbm.1, bf16[256,2048]{1,0:T(8,128)(2,1)} %res_hbm.1, ...), custom_call_target="tpu_custom_call" | custom-call | tf_op jit(solution)/shard_map/pallas_call | solution.py:450
  163.1 2.3 %copy.29 = bf16[256,2048]{1,0:T(8,128)(2,1)} copy(bf16[256,2048]{1,0:T(8,128)(2,1)} %shard_map.154) | data formatting | bytes 2097152
  (3 shorter events, 0.0 us)

commit v2 on v1

--- a/solution.py
+++ b/solution.py
@@ -9,8 +9,8 @@
 
 epsilon = 1e-06
 masked_score = -1e30
-EXTRA = 32
-KV, GATE, VALUE, DOWN = range(4)
+EXTRA = 16
+GATE, VALUE, DOWN = range(3)
 
 
 def kernel(
@@ -56,6 +56,10 @@
     local_sem,
     ring_send,
     ring_recv,
+    up_send,
+    up_recv,
+    rung_send,
+    rung_recv,
     nrm_send,
     nrm_recv,
     halo_send,
@@ -85,12 +89,7 @@
     neighbour = (at(pos + 1), at(pos - 1))
 
     def place(kind, owner, piece):
-        if kind == KV:
-            size = kvb.shape[1]
-            if piece is None:
-                return kvb.at[owner]
-            return kvb.at[owner, pl.ds(piece * (size // 2), size // 2)]
-        ref = (None, gb, vb, db)[kind]
+        ref = (gb, vb, db)[kind]
         if piece is None:
             return ref.at[pl.ds(pl.multiple_of(owner * rows, rows), rows)]
         return ref.at[pl.ds(pl.multiple_of(owner * rows + piece * (rows // 2), rows // 2), rows // 2)]
@@ -130,21 +129,6 @@
     ]
     for copy in local:
         copy.start()
-    local[0].wait()
-    for way in range(2):
-        send(KV, way, 1)
-    for step in range(1, half):
-        for way in range(2):
-            arrive(KV, way, step)
-            send(KV, way, step + 1)
-    for i in (1, 2, 3):
-        local[i].wait()
-    for kind in (GATE, VALUE, DOWN):
-        for way in range(2):
-            send(kind, way, 1)
-    for way in range(2):
-        arrive(KV, way, half)
-
     mrow[...] = jnp.full(mrow.shape, masked_score, jnp.float32)
     lrow[...] = jnp.zeros(lrow.shape, jnp.float32)
     att[...] = jnp.zeros(att.shape, jnp.float32)
@@ -154,8 +138,7 @@
         jnp.int32, (tok, tok), 1
     )
 
-    @pl.loop(0, jnp.minimum(s, half) + 1)
-    def _(back):
+    def attend(back):
         o = s - back
         doc_key = kvb[o, pl.ds(tok, 16), pl.ds(0, tok)].astype(jnp.float32)[0:1]
         allowed = (delta + back * tok >= 0) & (doc_key == doc_query)
@@ -173,7 +156,7 @@
                 idx = h * 2 + m
                 old = mrow[idx, :, 0:1]
                 new = jnp.maximum(old, jnp.max(scores, axis=1, keepdims=True))
-                probs = jnp.where(allowed, jnp.exp(scores - new), 0.0)
+                probs = jnp.exp(scores - new)
                 factor = jnp.exp(old - new)
                 total = lrow[idx, :, 0:1] * factor + jnp.sum(probs, axis=1, keepdims=True)
                 att[idx] = att[idx] * factor + jnp.dot(
@@ -181,6 +164,106 @@
                 )
                 mrow[idx] = jnp.broadcast_to(new, (tok, hd))
                 lrow[idx] = jnp.broadcast_to(total, (tok, hd))
+
+    def attend_if(back):
+        pl.when(s >= back)(functools.partial(attend, back))
+
+    depth = (half + 1) // 2
+    column, row = s % 2, s // 2
+    top = n // 2 - 1
+
+    def kv_copy(owner, target, send_sem, recv_sem):
+        ref = kvb.at[jnp.maximum(owner, 0)]
+        return pltpu.make_async_remote_copy(
+            src_ref=ref,
+            dst_ref=ref,
+            send_sem=send_sem,
+            recv_sem=recv_sem,
+            device_id={"sp": target},
+            device_id_type=pl.DeviceIdType.MESH,
+        )
+
+    def up(j, owner):
+        target = jnp.minimum(s + 2, n - 1)
+        return kv_copy(owner, target, up_send.at[j - 1], up_recv.at[j - 1])
+
+    def rung(i, owner):
+        return kv_copy(owner, s + 1 - 2 * column, rung_send.at[i], rung_recv.at[i])
+
+    def up_sends(j):
+        return (row < top) & (row - (j - 1) >= 0)
+
+    def start_up(j):
+        @pl.when(up_sends(j))
+        def _():
+            up(j, s - 2 * (j - 1)).start()
+
+    def wait_up(j):
+        @pl.when(row >= j)
+        def _():
+            up(j, s - 2 * j).wait_recv()
+
+    def rung_owner(i):
+        return s - 2 * i - 2 * column
+
+    def start_rung(i, only):
+        @pl.when((column == only) & (rung_owner(i) >= 0))
+        def _():
+            rung(i, rung_owner(i)).start()
+
+    def wait_rung(i):
+        @pl.when(s - 1 - 2 * i >= 0)
+        def _():
+            rung(i, s - 1 - 2 * i).wait_recv()
+
+    def send_own(way):
+        for kind in (GATE, VALUE, DOWN):
+            send(kind, way, 1)
+
+    local[0].wait()
+    start_up(1)
+    start_rung(0, 0)
+    for i in (1, 2, 3):
+        local[i].wait()
+
+    @pl.when(column == 0)
+    def _():
+        send_own(1)
+
+    @pl.when(column == 1)
+    def _():
+        send_own(0)
+
+    near = depth <= 2
+    if near:
+        attend(0)
+    for j in range(1, depth + 1):
+        wait_up(j)
+        if j < depth:
+            start_up(j + 1)
+            start_rung(j, 0)
+        start_rung(j - 1, 1)
+        if j == max(depth - 1, 1):
+
+            @pl.when(column == 0)
+            def _():
+                send_own(0)
+
+            @pl.when(column == 1)
+            def _():
+                send_own(1)
+
+        if near:
+            attend_if(2 * j)
+    for i in range(depth):
+        wait_rung(i)
+        if near:
+            attend_if(2 * i + 1)
+    if not near:
+
+        @pl.loop(0, jnp.minimum(s, 2 * depth) + 1)
+        def _(back):
+            attend(back)
 
     for h in range(heads):
         head = att[2 * h] / lrow[2 * h] - lam_ref[h] * (att[2 * h + 1] / lrow[2 * h + 1])
@@ -202,6 +285,14 @@
 
     for i in range(1, ntp):
         nrm_copy(i, t).start()
+
+    def pass_on(kind, step):
+        for way in range(2):
+            arrive(kind, way, step)
+            if step < half:
+                send(kind, way, step + 1)
+
+    pass_on(GATE, 1)
     local[4].wait()
     local[5].wait()
     for i in range(1, ntp):
@@ -219,6 +310,8 @@
             )
         stream[:, cols] = acc
 
+    pass_on(VALUE, 1)
+
     def rms(x, gain):
         return x * lax.rsqrt(jnp.mean(x * x, axis=1, keepdims=True) + epsilon) * gain
 
@@ -247,14 +340,10 @@
             add_block(kind, s, True)
     for step in range(1, half + 1):
         for kind in (GATE, VALUE):
-            for way in range(2):
-                arrive(kind, way, step)
-                if step < half:
-                    send(kind, way, step + 1)
+            if step > 1:
+                pass_on(kind, step)
             if step == half and kind == VALUE:
-                for way in range(2):
-                    arrive(DOWN, way, 1)
-                    send(DOWN, way, 2)
+                pass_on(DOWN, 1)
             if fine:
                 add_block(kind, came(0, step), False)
                 if step < half:
@@ -373,25 +462,39 @@
 
     mine = pl.multiple_of(t * share, share)
 
-    @pl.loop(0, share // chunk)
-    def _(c):
+    pair = ntp == 4
+    sibling = jnp.where(t % 2 == 0, 1, ntp - 1)
+    turns = [ntp // 2, sibling] if pair else list(range(1, ntp))
+    lumps = share // chunk
+
+    def ag_copy(turn, sem, owner, c):
+        ref = out_ref.at[pl.ds(pl.multiple_of(owner * share + c * chunk, chunk), chunk)]
+        return peer_copy(ref, ref, ag_send.at[sem, c], ag_recv.at[sem, c], turn)
+
+    for c in range(lumps):
         at_rows = pl.ds(pl.multiple_of(mine + c * chunk, chunk), chunk)
-        in_rows = pl.ds(pl.multiple_of(c * chunk, chunk), chunk)
+        in_rows = pl.ds(c * chunk, chunk)
         lifted = part[at_rows].astype(jnp.float32)
         for i in range(1, ntp):
             lifted = lifted + rsb[i - 1, in_rows].astype(jnp.float32)
         out_ref[at_rows] = (stream[at_rows] + rms(lifted, mlpg_ref[...])).astype(jnp.bfloat16)
-
-    def ag_copy(i, owner):
-        ref = out_ref.at[pl.ds(pl.multiple_of(owner * share, share), share)]
-        return peer_copy(ref, ref, ag_send.at[i], ag_recv.at[i], i)
-
-    for i in range(1, ntp):
-        ag_copy(i, t).start()
-    for i in range(1, ntp):
-        ag_copy(i, (t - i + ntp) % ntp).wait_recv()
-
-    for kind in (KV, GATE, VALUE, DOWN):
+        for sem, turn in enumerate(turns):
+            ag_copy(turn, sem, t, c).start()
+    opposite = (t + ntp // 2) % ntp
+    beside = (t + sibling) % ntp
+    if pair:
+        for c in range(lumps):
+            ag_copy(turns[0], 0, opposite, c).wait_recv()
+            ag_copy(sibling, 2, opposite, c).start()
+        for c in range(lumps):
+            ag_copy(sibling, 1, beside, c).wait_recv()
+            ag_copy(sibling, 2, (beside + ntp // 2) % ntp, c).wait_recv()
+    else:
+        for c in range(lumps):
+            for sem, turn in enumerate(turns):
+                ag_copy(turn, sem, (t - turn + ntp) % ntp, c).wait_recv()
+
+    for kind in (GATE, VALUE, DOWN):
         for way in range(2):
             for step in range(1, half + 1):
                 hop(kind, way, step, came(way, step - 1)).wait_send()
@@ -399,7 +502,20 @@
         nrm_copy(i, t).wait_send()
         for b, cols in pieces:
             rs_copy(i, b, cols).wait_send()
-        ag_copy(i, t).wait_send()
+    for c in range(lumps):
+        for sem, turn in enumerate(turns):
+            ag_copy(turn, sem, t, c).wait_send()
+        if pair:
+            ag_copy(sibling, 2, opposite, c).wait_send()
+    for j in range(1, depth + 1):
+
+        @pl.when(up_sends(j))
+        def _():
+            up(j, s - 2 * (j - 1)).wait_send()
+
+        @pl.when(rung_owner(j - 1) >= 0)
+        def _():
+            rung(j - 1, rung_owner(j - 1)).wait_send()
 
     @pl.when(s < n - 1)
     def _():
@@ -475,16 +591,20 @@
             pltpu.VMEM((2 * heads, tok, hd), f32),
             pltpu.VMEM((2 * heads, tok, hd), f32),
             dma((6,)),
-            dma((4, 2, half)),
-            dma((4, 2, half)),
+            dma((3, 2, half)),
+            dma((3, 2, half)),
+            dma((half,)),
+            dma((half,)),
+            dma((half,)),
+            dma((half,)),
             dma((ntp,)),
             dma((ntp,)),
             dma,
             dma,
             dma((n, ntp)),
             dma((n, ntp)),
-            dma((ntp,)),
-            dma((ntp,)),
+            dma((ntp, share // 16)),
+            dma((ntp, share // 16)),
         ],
         compiler_params=pltpu.CompilerParams(
             has_side_effects=True, vmem_limit_bytes=60 * 1024 * 1024

time: 167 us -> 153 us (0.916)
  Pallas kernels: 158 us -> 144 us
    pallas_call x1, Pallas kernels: 158 us -> 144 us  [per_device(): pl.pallas_call(functools.partial(kernel, n, ntp), out_shape=jax.ShapeDtyp...]
where the time goes in v2:
time: 153 us; the launch traced here: 151 us
  Pallas kernels  144 us (94%)
  local copies, waits for them, and re-layouts  4.86 us (3%)
  other arithmetic  2.52 us (2%)
    pallas_call x1, Pallas kernels, per_device(): pl.pallas_call(functools.partial(kernel, n, ntp), out_shape=jax.ShapeDtyp...  144 us

profile of v2, /device:TPU:0, one launch (start us, length us, event | category | flops | bytes accessed | tf_op | source)
XLA Modules:
  0.0 151.4 jit_solution(2309945494691914333)
XLA Ops:
  0.0 0.7 fusion
  0.7 0.1 concatenate.15
  0.8 0.1 pad_maximum_fusion.2
  0.9 0.1 copy.20
  1.0 0.7 pad.11.dcol_ref
  1.7 1.0 multiply_convert_fusion
  2.7 0.7 copy.27
  3.4 1.0 copy_bitcast_fusion.1
  4.4 0.7 pad_maximum_fusion.kv_hbm
  5.1 144.0 %shard_map.154 = bf16[256,2048]{1,0:T(8,128)(2,1)} custom-call(f32[2]{0:T(128)} %lam_ref.1, bf16[272,512]{1,0:T(8,128)(2,1)} %pad_maximum_fusion.kv_hbm, bf16[256,768]{1,0:T(8,128)(2,1)} %g_hbm.1, bf16[256,768]{1,0:T(8,128)(2,1)} %v_hbm.1, bf16[256,768]{1,0:T(8,128)(2,1)} %d_hbm.1, bf16[1024,2048]{1,0:T(8,128)(2,1)} %ow_hbm.1, bf16[256,2048]{1,0:T(8,128)(2,1)} %res_hbm.1, ...), custom_call_target="tpu_custom_call" | custom-call | tf_op jit(solution)/shard_map/pallas_call | solution.py:566
  149.1 2.3 %copy.29 = bf16[256,2048]{1,0:T(8,128)(2,1)} copy(bf16[256,2048]{1,0:T(8,128)(2,1)} %shard_map.154) | data formatting | bytes 2097152
  (3 shorter events, 0.0 us)

commit v3 on v2

--- a/solution.py
+++ b/solution.py
@@ -10,21 +10,22 @@
 epsilon = 1e-06
 masked_score = -1e30
 EXTRA = 16
-GATE, VALUE, DOWN = range(3)
+GATE, VALUE, DOWN, DOWN2 = range(4)
 
 
 def kernel(
     n,
     ntp,
     lam_ref,
-    kv_hbm,
+    k_ref,
+    v_ref,
     g_hbm,
     v_hbm,
     d_hbm,
     ow_hbm,
     res_hbm,
     q_ref,
-    dcol_ref,
+    doc_ref,
     hg_ref,
     mixg_ref,
     preg_ref,
@@ -32,6 +33,7 @@
     vt_ref,
     mlpg_ref,
     out_ref,
+    qs,
     kvb,
     gb,
     vb,
@@ -89,13 +91,16 @@
     neighbour = (at(pos + 1), at(pos - 1))
 
     def place(kind, owner, piece):
-        ref = (gb, vb, db)[kind]
+        ref = (gb, vb, db, db)[kind]
         if piece is None:
             return ref.at[pl.ds(pl.multiple_of(owner * rows, rows), rows)]
         return ref.at[pl.ds(pl.multiple_of(owner * rows + piece * (rows // 2), rows // 2), rows // 2)]
 
     def hop(kind, way, step, owner):
-        ref = place(kind, owner, way if step == half else None)
+        piece = way if step == half else None
+        if kind >= DOWN:
+            piece = kind - DOWN
+        ref = place(kind, owner, piece)
         return pltpu.make_async_remote_copy(
             src_ref=ref,
             dst_ref=ref,
@@ -108,17 +113,21 @@
     def came(way, step):
         return at(pos - step) if way == 0 else at(pos + step)
 
+    def used(kind, way, step):
+        return kind < DOWN or step < half or kind - DOWN == way
+
     def send(kind, way, step):
-        hop(kind, way, step, came(way, step - 1)).start()
+        if used(kind, way, step):
+            hop(kind, way, step, came(way, step - 1)).start()
 
     def arrive(kind, way, step):
-        hop(kind, way, step, came(way, step)).wait_recv()
+        if used(kind, way, step):
+            hop(kind, way, step, came(way, step)).wait_recv()
 
     local = [
         pltpu.make_async_copy(src, dst, local_sem.at[i])
         for i, (src, dst) in enumerate(
             (
-                (kv_hbm, kvb.at[s]),
                 (g_hbm, place(GATE, s, None)),
                 (v_hbm, place(VALUE, s, None)),
                 (d_hbm, place(DOWN, s, None)),
@@ -132,7 +141,14 @@
     mrow[...] = jnp.full(mrow.shape, masked_score, jnp.float32)
     lrow[...] = jnp.zeros(lrow.shape, jnp.float32)
     att[...] = jnp.zeros(att.shape, jnp.float32)
-    doc_query = dcol_ref[:, 0:1]
+    on_row = lax.broadcasted_iota(jnp.int32, (tok, tok), 0)
+    on_lane = lax.broadcasted_iota(jnp.int32, (tok, tok), 1)
+
+    def doc_before(shift):
+        spread = jnp.broadcast_to(doc_ref[...].astype(jnp.float32), (tok, tok))
+        return jnp.sum(jnp.where(on_row - shift == on_lane, spread, 0.0), axis=1, keepdims=True)
+
+    doc_query = doc_before(0)
     lane = lax.broadcasted_iota(jnp.int32, (tok, hd), 1)
     delta = lax.broadcasted_iota(jnp.int32, (tok, tok), 0) - lax.broadcasted_iota(
         jnp.int32, (tok, tok), 1
@@ -145,7 +161,7 @@
         for h in range(heads):
             k = kvb[o, pl.ds(0, tok), pl.ds(h * hd, hd)]
             val = kvb[o, pl.ds(0, tok), pl.ds(hw + h * hd, hd)]
-            qh = q_ref[:, h * hd : (h + 1) * hd]
+            qh = qs[:, h * hd : (h + 1) * hd]
             for m in range(2):
                 keep = lane < hd // 2 if m == 0 else lane >= hd // 2
                 qm = jnp.where(keep, qh, jnp.zeros_like(qh))
@@ -216,23 +232,31 @@
         def _():
             rung(i, s - 1 - 2 * i).wait_recv()
 
-    def send_own(way):
-        for kind in (GATE, VALUE, DOWN):
-            send(kind, way, 1)
-
-    local[0].wait()
+    def send_own(free_way, kinds):
+        for c in range(2):
+
+            @pl.when(column == c)
+            def _():
+                for kind in kinds:
+                    send(kind, free_way if c == 0 else 1 - free_way, 1)
+
+    for i in (0, 1, 2):
+        local[i].wait()
+    send_own(1, (GATE, VALUE, DOWN, DOWN2))
+    doc_row = doc_ref[...].astype(jnp.float32)
+    kvb[s, pl.ds(tok, 16), pl.ds(0, tok)] = jnp.broadcast_to(doc_row, (16, tok)).astype(
+        jnp.bfloat16
+    )
+    for h in range(heads):
+        kvb[s, pl.ds(0, tok), pl.ds(h * hd, hd)] = k_ref[:, h, :]
+        kvb[s, pl.ds(0, tok), pl.ds(hw + h * hd, hd)] = v_ref[:, h, :]
+    for h in range(heads):
+        qs[:, h * hd : (h + 1) * hd] = (
+            q_ref[:, h, :].astype(jnp.float32) * (hd // 2) ** (-0.5)
+        ).astype(jnp.bfloat16)
     start_up(1)
     start_rung(0, 0)
-    for i in (1, 2, 3):
-        local[i].wait()
-
-    @pl.when(column == 0)
-    def _():
-        send_own(1)
-
-    @pl.when(column == 1)
-    def _():
-        send_own(0)
+    send_own(0, (GATE,))
 
     near = depth <= 2
     if near:
@@ -244,15 +268,7 @@
             start_rung(j, 0)
         start_rung(j - 1, 1)
         if j == max(depth - 1, 1):
-
-            @pl.when(column == 0)
-            def _():
-                send_own(0)
-
-            @pl.when(column == 1)
-            def _():
-                send_own(1)
-
+            send_own(0, (VALUE, DOWN, DOWN2))
         if near:
             attend_if(2 * j)
     for i in range(depth):
@@ -293,8 +309,8 @@
                 send(kind, way, step + 1)
 
     pass_on(GATE, 1)
+    local[3].wait()
     local[4].wait()
-    local[5].wait()
     for i in range(1, ntp):
         nrm_copy(i, (t - i + ntp) % ntp).wait_recv()
 
@@ -344,6 +360,7 @@
                 pass_on(kind, step)
             if step == half and kind == VALUE:
                 pass_on(DOWN, 1)
+                pass_on(DOWN2, 1)
             if fine:
                 add_block(kind, came(0, step), False)
                 if step < half:
@@ -386,8 +403,8 @@
     last1 = jnp.where(has_prev, last1, -1.0)
     last2 = jnp.where(has_prev, last2, -1.0)
     rowid = lax.broadcasted_iota(jnp.int32, (tok, 1), 0)
-    doc1 = jnp.where(rowid == 0, last1, dcol_ref[:, 1:2])
-    doc2 = jnp.where(rowid == 0, last2, jnp.where(rowid == 1, last1, dcol_ref[:, 2:3]))
+    doc1 = jnp.where(rowid == 0, last1, doc_before(1))
+    doc2 = jnp.where(rowid == 0, last2, jnp.where(rowid == 1, last1, doc_before(2)))
     same1 = doc1 == doc_query
     same2 = doc2 == doc_query
 
@@ -430,11 +447,9 @@
     if fine:
         down_block(s, 0)
     for step in range(1, half + 1):
-        for way in range(2):
-            if step > 1:
-                arrive(DOWN, way, step)
-                if step < half:
-                    send(DOWN, way, step + 1)
+        if step > 1:
+            pass_on(DOWN, step)
+            pass_on(DOWN2, step)
         for way in range(2 if step < half else 1):
             if fine:
                 down_block(came(way, step), len(order))
@@ -494,10 +509,11 @@
             for sem, turn in enumerate(turns):
                 ag_copy(turn, sem, (t - turn + ntp) % ntp, c).wait_recv()
 
-    for kind in (GATE, VALUE, DOWN):
+    for kind in range(4):
         for way in range(2):
             for step in range(1, half + 1):
-                hop(kind, way, step, came(way, step - 1)).wait_send()
+                if used(kind, way, step):
+                    hop(kind, way, step, came(way, step - 1)).wait_send()
     for i in range(1, ntp):
         nrm_copy(i, t).wait_send()
         for b, cols in pieces:
@@ -548,16 +564,6 @@
     rows, ff = gate_weight.shape
     half = n // 2
     share = tok // ntp
-    docs = documents.astype(jnp.float32)
-    packed = jnp.concatenate([keys.reshape(tok, hw), values.reshape(tok, hw)], axis=1)
-    doc_rows = jnp.broadcast_to(
-        jnp.pad(docs, (0, 2 * hw - tok)).astype(jnp.bfloat16)[None, :], (EXTRA, 2 * hw)
-    )
-    kv = jnp.concatenate([packed, doc_rows], axis=0)
-    back = [jnp.concatenate([jnp.full((j,), -1.0, jnp.float32), docs[: tok - j]]) for j in (1, 2)]
-    dcol = jnp.pad(jnp.stack([docs] + back, axis=1), ((0, 0), (0, 125)))
-    score_scale = (hd // 2) ** (-0.5)
-    q = (queries.astype(jnp.float32) * score_scale).astype(jnp.bfloat16).reshape(tok, hw)
     bf, f32 = jnp.bfloat16, jnp.float32
     vm = pl.BlockSpec(memory_space=pltpu.VMEM)
     hbm = pl.BlockSpec(memory_space=pl.ANY)
@@ -566,9 +572,10 @@
     return pl.pallas_call(
         functools.partial(kernel, n, ntp),
         out_shape=jax.ShapeDtypeStruct((tok, width), bf),
-        in_specs=[smem] + [hbm] * 6 + [vm] * 8,
+        in_specs=[smem] + [vm] * 2 + [hbm] * 5 + [vm] * 8,
         out_specs=vm,
         scratch_shapes=[
+            pltpu.VMEM((tok, hw), bf),
             pltpu.VMEM((n, tok + EXTRA, 2 * hw), bf),
             pltpu.VMEM((n * rows, ff), bf),
             pltpu.VMEM((n * rows, ff), bf),
@@ -591,8 +598,8 @@
             pltpu.VMEM((2 * heads, tok, hd), f32),
             pltpu.VMEM((2 * heads, tok, hd), f32),
             dma((6,)),
-            dma((3, 2, half)),
-            dma((3, 2, half)),
+            dma((4, 2, half)),
+            dma((4, 2, half)),
             dma((half,)),
             dma((half,)),
             dma((half,)),
@@ -611,14 +618,15 @@
         ),
     )(
         lambdas,
-        kv,
+        keys,
+        values,
         gate_weight,
         value_weight,
         down_weight,
         out_weight,
         residual,
-        q,
-        dcol,
+        queries,
+        documents[None],
         head_gain,
         mix_gain[None],
         pre_gain[None],

time: 153 us -> 145 us (0.948)
  Pallas kernels: 144 us -> 140 us
  local copies, waits for them, and re-layouts: 4.86 us -> 2.3 us
  other arithmetic: 2.52 us -> 0 us
    pallas_call x1, Pallas kernels: 144 us -> 140 us  [per_device(): pl.pallas_call(functools.partial(kernel, n, ntp), out_shape=jax.ShapeDtyp...]
    convert_element_type x2 -> x0, other arithmetic: 1.7 us -> none  [the longest x1 1.02 us: per_device(): (queries.astype(jnp.float32) * score_scale).astype(jnp.bfloat16)]
where the time goes in v3:
time: 145 us; the launch traced here: 142 us
  Pallas kernels  140 us (97%)
  local copies, waits for them, and re-layouts  2.3 us (2%)
    pallas_call x1, Pallas kernels, per_device(): pl.pallas_call(functools.partial(kernel, n, ntp), out_shape=jax.ShapeDtyp...  140 us

profile of v3, /device:TPU:0, one launch (start us, length us, event | category | flops | bytes accessed | tf_op | source)
XLA Modules:
  0.0 142.1 jit_solution(15986720789483551925)
XLA Ops:
  0.0 139.8 %shard_map.154 = bf16[256,2048]{1,0:T(8,128)(2,1)} custom-call(f32[2]{0:T(128)} %lam_ref.1, bf16[256,2,128]{2,1,0:T(2,128)(2,1)} %k_ref.1, bf16[256,2,128]{2,1,0:T(2,128)(2,1)} %v_ref.1, bf16[256,768]{1,0:T(8,128)(2,1)} %g_hbm.1, bf16[256,768]{1,0:T(8,128)(2,1)} %v_hbm.1, bf16[256,768]{1,0:T(8,128)(2,1)} %d_hbm.1, bf16[1024,2048]{1,0:T(8,128)(2,1)} %ow_hbm.1, ...), custom_call_target="tpu_custom_call" | custom-call | tf_op jit(solution)/shard_map/pallas_call | solution.py:572
  139.8 2.3 %copy.18 = bf16[256,2048]{1,0:T(8,128)(2,1)} copy(bf16[256,2048]{1,0:T(8,128)(2,1)} %shard_map.154) | data formatting | bytes 2097152
